TPU v7x, 32 devices: a whole 2x2x4 slice. The times are simulated.
32 devices in a mesh: fs: 16 (over z, y, core), tp: 2 (over x).
Axes of the slice: x: 2, y: 2, z: 4, core: 2. Of those that a mesh axis runs over, the one named last changes fastest.
Arguments:
- saved_input: bfloat16 [8192, 3072], P('fs'), may hold values from -6 to 6
- output_cotangent: bfloat16 [8192, 3072], P('fs'), may hold values from -6 to 6
- recurrent_output: bfloat16 [8192, 1536], P('fs', 'tp'), may hold values from -6 to 6
- forget_logit: bfloat16 [8192, 1536], P('fs', 'tp'), may hold values from -12 to 12
- forget_cotangent: bfloat16 [8192, 1536], P('fs', 'tp'), may hold values from -6 to 6
- lower_bound: float32 [1536], P('tp'), may hold values from 0.2 to 0.9
- basis_in: bfloat16 [3072, 384], P('fs'), may hold values from -1.2629537 to 1.2629537
- basis_out: bfloat16 [3072, 384], P('fs'), may hold values from -1.2629537 to 1.2629537
- moment_in: float32 [384, 1536], P('fs', 'tp'), may hold values from -6 to 6
- second_in: float32 [384, 1536], P('fs', 'tp'), may hold values from 0.25 to 4
- moment_out: float32 [384, 1536], P('fs', 'tp'), may hold values from -6 to 6
- second_out: float32 [384, 1536], P('fs', 'tp'), may hold values from 0.25 to 4
- weight_in: float32 [3072, 1536], P('fs', 'tp'), may hold values from -0.109375 to 0.109375
- weight_out: float32 [1536, 3072], P('tp', 'fs'), may hold values from -0.15625 to 0.15625
Outputs:
- moment_in_new: float32 [384, 1536], P('fs', 'tp')
- second_in_new: float32 [384, 1536], P('fs', 'tp')
- moment_out_new: float32 [384, 1536], P('fs', 'tp')
- second_out_new: float32 [384, 1536], P('fs', 'tp')
- weight_in_new: float32 [3072, 1536], P('fs', 'tp')
- weight_out_new: float32 [1536, 3072], P('tp', 'fs')
- copy_in: bfloat16 [3072, 1536], P(None, 'tp')
- copy_out: bfloat16 [1536, 3072], P('tp')
All inputs are finite; a program needn't handle non-finite values.
Results may differ from a plain program's by a relative error of at most 0.0023.
Values may be sent and summed in bfloat16 or wider, within the bound.
A program may use at most 64 MiB of HBM per device.

v0:
```python
import jax
import jax.numpy as jnp
from jax import lax
from jax.sharding import PartitionSpec as P

HW = 1536
R = 384


def body(
    saved_input,
    output_cotangent,
    recurrent_output,
    forget_logit,
    forget_cotangent,
    lower_bound,
    basis_in,
    basis_out,
    moment_in,
    second_in,
    moment_out,
    second_out,
    weight_in,
    weight_out,
):
    sig = jax.nn.sigmoid(forget_logit.astype(jnp.float32))
    gate_cot = (
        forget_cotangent.astype(jnp.float32) * (1.0 - lower_bound)[None, :] * sig * (1.0 - sig)
    ).astype(jnp.bfloat16)
    full_in, full_out = (
        lax.all_gather(basis_in, "fs", axis=0, tiled=True),
        lax.all_gather(basis_out, "fs", axis=0, tiled=True),
    )
    coded_in = jnp.dot(saved_input, full_in, preferred_element_type=jnp.float32).astype(
        jnp.bfloat16
    )
    coded_out = jnp.dot(output_cotangent, full_out, preferred_element_type=jnp.float32).astype(
        jnp.bfloat16
    )
    units = recurrent_output.shape[1]
    contract = (((0,), (0,)), ((), ()))
    term_in = lax.dot_general(coded_in, gate_cot, contract, preferred_element_type=jnp.float32)
    term_out = lax.dot_general(
        coded_out, recurrent_output, contract, preferred_element_type=jnp.float32
    )
    lowrank = lax.psum_scatter(
        jnp.concatenate([term_in, term_out], axis=1), "fs", scatter_dimension=0, tiled=True
    )
    total = lax.psum(jnp.sum(lowrank * lowrank), ("fs", "tp"))
    clip = jnp.minimum(1.0, jnp.sqrt(jnp.float32(2 * R * HW)) * lax.rsqrt(total + 1e-06))
    grads = clip * lowrank
    moments = 0.8 * jnp.concatenate([moment_in, moment_out], axis=1) + 0.2 * grads
    seconds = 0.9 * jnp.concatenate([second_in, second_out], axis=1) + 0.1 * grads * grads
    stepping = moments / (jnp.sqrt(seconds) + 1e-08)
    whole_step = lax.all_gather(stepping, "fs", axis=0, tiled=True)
    update_in = jnp.dot(
        basis_in.astype(jnp.float32), whole_step[:, :units], precision=lax.Precision.HIGHEST
    )
    update_out = jnp.dot(
        whole_step[:, units:].T, basis_out.astype(jnp.float32).T, precision=lax.Precision.HIGHEST
    )
    weight_in_new = weight_in - 0.01 * update_in
    weight_out_new = weight_out - 0.01 * update_out
    copy_in, copy_out = (
        lax.all_gather(weight_in_new.astype(jnp.bfloat16), "fs", axis=0, tiled=True),
        lax.all_gather(weight_out_new.astype(jnp.bfloat16), "fs", axis=1, tiled=True),
    )
    return (
        moments[:, :units],
        seconds[:, :units],
        moments[:, units:],
        seconds[:, units:],
        weight_in_new,
        weight_out_new,
        copy_in,
        copy_out,
    )


def solution(mesh):
    return jax.shard_map(
        body,
        mesh=mesh,
        in_specs=(
            P("fs", None),
            P("fs", None),
            P("fs", "tp"),
            P("fs", "tp"),
            P("fs", "tp"),
            P("tp"),
            P("fs", None),
            P("fs", None),
            P("fs", "tp"),
            P("fs", "tp"),
            P("fs", "tp"),
            P("fs", "tp"),
            P("fs", "tp"),
            P("tp", "fs"),
        ),
        out_specs=(
            P("fs", "tp"),
            P("fs", "tp"),
            P("fs", "tp"),
            P("fs", "tp"),
            P("fs", "tp"),
            P("tp", "fs"),
            P(None, "tp"),
            P("tp", None),
        ),
        check_vma=False,
    )
```

profile of v0, /device:TPU:0, one launch (start us, length us, event | category | flops | bytes accessed | tf_op | source)
XLA Modules:
  0.0 377.6 jit_solution(13971637352224902390)
XLA Ops:
  7.2 0.7 all-gather.8.cloned.1.call-update
  8.0 0.7 all-gather.6.cloned.1.call-update
  8.7 0.0 reduce-scatter.2.cloned.1.call-start
  8.7 0.7 broadcast_subtract_fusion
  9.4 45.9 %all-gather.8.cloned.1.call-done = bf16[3072,384]{1,0:T(8,128)(2,1)} async-done(((bf16[192,384]{1,0:T(8,128)(2,1)}), bf16[3072,384]{1,0:T(8,128)(2,1)}) %all-gather.8.cloned.1.call-update) | async-done | bytes 2359312 | tf_op jit(solution)/shard_map/all_gather | solution.py:32
  55.3 5.2 %fusion.6 = f32[384,768]{1,0:T(8,128)} fusion(bf16[512,768]{1,0:T(8,128)(2,1)} %param.16, bf16[512,3072]{1,0:T(8,128)(2,1)S(1)} %copy-done, bf16[3072,384]{1,0:T(8,128)(2,1)} %all-gather.8.cloned.1.call-done), kind=kOutput, calls=%fused_computation.12 | convolution fusion | flops 1510146048 | bytes 7471104 | tf_op jit(solution)/shard_map/dot_general | solution.py:43
  60.5 38.1 %all-gather.6.cloned.1.call-done = bf16[3072,384]{1,0:T(8,128)(2,1)} async-done(((bf16[192,384]{1,0:T(8,128)(2,1)}), bf16[3072,384]{1,0:T(8,128)(2,1)}) %all-gather.6.cloned.1.call-update) | async-done | bytes 2359312 | tf_op jit(solution)/shard_map/all_gather | solution.py:31
  98.7 6.5 %fusion.5 = f32[384,768]{1,0:T(8,128)} fusion(bf16[512,3072]{1,0:T(8,128)(2,1)} %param.14, bf16[3072,384]{1,0:T(8,128)(2,1)} %all-gather.6.cloned.1.call-done, bf16[512,768]{1,0:T(8,128)(2,1)} %param.17, bf16[512,768]{1,0:T(8,128)(2,1)} %param.18, f32[768]{0:T(1024)S(1)} %broadcast_subtract_fusion), kind=kOutput, calls=%fused_computation.11 | convolution fusion | flops 1514078208 | bytes 8260608 | tf_op jit(solution)/shard_map/dot_general | solution.py:42
  105.2 3.3 pad_maximum_fusion
  108.5 0.0 all-gather.10.cloned.1.call-start
  108.5 62.0 %reduce-scatter.2.cloned.1.call-done = f32[24,1536]{1,0:T(8,128)} async-done(((f32[384,1536]{1,0:T(8,128)}), f32[24,1536]{1,0:T(8,128)}) %reduce-scatter.2.cloned.1.call-update) | async-done | bytes 147472 | tf_op jit(solution)/shard_map/reduce_scatter | solution.py:46
  170.6 1.6 multiply_reduce_fusion
  172.1 40.0 %psum.7 = f32[]{:T(128)} all-reduce(f32[]{:T(128)} %multiply_reduce_fusion), channel_id=1, replica_groups=mesh['fs'=16,'tp'=2] {'fs','tp'}, use_global_device_ids=true, to_apply=%region_2.0 | all-reduce | flops 1 | bytes 8 | tf_op jit(solution)/shard_map/psum | solution.py:49
  212.8 1.8 add_divide_fusion
  214.6 0.0 all-gather.14.cloned.1.call-start
  214.7 41.8 %all-gather.10.cloned.1.call-done = f32[384,1536]{1,0:T(8,128)} async-done(((f32[24,1536]{1,0:T(8,128)}), f32[384,1536]{1,0:T(8,128)}) %all-gather.10.cloned.1.call-update) | async-done | bytes 2359312 | tf_op jit(solution)/shard_map/all_gather | solution.py:55
  256.5 3.0 fusion.16
  259.5 0.0 all-gather.12.cloned.1.call-start
  259.6 3.0 fusion.15
  262.6 1.6 fusion.13
  264.3 47.2 %all-gather.14.cloned.1.call-done = bf16[768,3072]{0,1:T(8,128)(2,1)} async-done(((bf16[768,192]{0,1:T(8,128)(2,1)}), bf16[768,3072]{0,1:T(8,128)(2,1)}) %all-gather.14.cloned.1.call-update) | async-done | bytes 4718608 | tf_op jit(solution)/shard_map/all_gather | solution.py:66
  311.5 6.6 %copy.22 = bf16[768,3072]{1,0:T(8,128)(2,1)} copy(bf16[768,3072]{0,1:T(8,128)(2,1)} %all-gather.14.cloned.1.call-done) | data formatting | bytes 9437184
  318.1 47.8 %all-gather.12.cloned.1.call-done = bf16[3072,768]{1,0:T(8,128)(2,1)} async-done(((bf16[192,768]{1,0:T(8,128)(2,1)}), bf16[3072,768]{1,0:T(8,128)(2,1)}) %all-gather.12.cloned.1.call-update) | async-done | bytes 4718608 | tf_op jit(solution)/shard_map/all_gather | solution.py:65
  365.9 4.8 %copy.24 = bf16[3072,768]{1,0:T(8,128)(2,1)} copy(bf16[3072,768]{1,0:T(8,128)(2,1)} %all-gather.12.cloned.1.call-done) | data formatting | bytes 9437184
  (16 shorter events, 0.2 us)
Async XLA Ops:
  7.2 48.2 %copy-start = (bf16[512,3072]{1,0:T(8,128)(2,1)S(1)}, bf16[512,3072]{1,0:T(8,128)(2,1)}, u32[]{:S(2)}) copy-start(bf16[512,3072]{1,0:T(8,128)(2,1)} %param.15) | copy-start | bytes 9437188
  7.2 48.2 %all-gather.8.cloned.1.call-start = ((), (), s32[]{:S(2)}) async-start(), calls=%async_computation.2 | async-start | bytes 2506752 | tf_op jit(solution)/shard_map/all_gather | solution.py:32
  7.9 90.8 %all-gather.6.cloned.1.call-start = ((), (), s32[]{:S(2)}) async-start(), calls=%async_computation.1 | async-start | bytes 2506752 | tf_op jit(solution)/shard_map/all_gather | solution.py:31
  8.7 161.9 %reduce-scatter.2.cloned.1.call-start = ((), (), s32[]{:S(2)}) async-start(), calls=%async_computation.3 | async-start | bytes 2506752 | tf_op jit(solution)/shard_map/reduce_scatter | solution.py:46
  108.4 104.3 %copy-start.4 = (f32[24,768]{1,0:T(8,128)S(1)}, f32[24,768]{1,0:T(8,128)}, u32[]{:S(2)}) copy-start(f32[24,768]{1,0:T(8,128)} %param.25) | copy-start | bytes 221188
  108.5 148.0 %copy-start.1 = (bf16[192,384]{1,0:T(8,128)(2,1)S(1)}, bf16[192,384]{1,0:T(8,128)(2,1)}, u32[]{:S(2)}) copy-start(bf16[192,384]{1,0:T(8,128)(2,1)} %param.21) | copy-start | bytes 442372
  108.5 151.1 %copy-start.2 = (bf16[192,384]{1,0:T(8,128)(2,1)S(1)}, bf16[192,384]{1,0:T(8,128)(2,1)}, u32[]{:S(2)}) copy-start(bf16[192,384]{1,0:T(8,128)(2,1)} %param.20) | copy-start | bytes 442372
  108.5 148.0 %all-gather.10.cloned.1.call-start = ((), (), s32[]{:S(2)}) async-start(), calls=%async_computation.4 | async-start | bytes 2506752 | tf_op jit(solution)/shard_map/all_gather | solution.py:55
  214.6 96.9 %all-gather.14.cloned.1.call-start = ((), (), s32[]{:S(2)}) async-start(), calls=%async_computation.6 | async-start | bytes 5013504 | tf_op jit(solution)/shard_map/all_gather | solution.py:66
  259.5 3.1 copy-start.3
  259.5 106.4 %all-gather.12.cloned.1.call-start = ((), (), s32[]{:S(2)}) async-start(), calls=%async_computation.5 | async-start | bytes 5013504 | tf_op jit(solution)/shard_map/all_gather | solution.py:65
Sparse Core Ops, SparseCore 0:
  10.3 45.0 all-gather.7
  57.6 41.0 all-gather.5
  108.6 61.9 reduce-scatter.1
  214.8 41.6 all-gather.9
  259.6 51.8 all-gather.13
  314.2 51.6 all-gather.11
where the time goes:
time: 378 us
  waiting for transfers between devices  284 us (75%)
  blocking collectives  40 us (11%)
  matrix products  17.7 us (5%)
  between operations  14.9 us (4%)
  local copies, waits for them, and re-layouts  13.1 us (3%)
  other arithmetic  7.34 us (2%)
    reduce_scatter x1, waiting for transfers between devices, body(): lax.psum_scatter(jnp.concatenate([term_in, term_out], axis=1), 'fs', scat...  62 us
    all_gather x1, waiting for transfers between devices, body(): lax.all_gather(weight_in_new.astype(jnp.bfloat16), 'fs', axis=0, tiled=True)  47.8 us
    all_gather x1, waiting for transfers between devices, body(): lax.all_gather(weight_out_new.astype(jnp.bfloat16), 'fs', axis=1, tiled=T...  47.2 us
    all_gather x1, waiting for transfers between devices, body(): lax.all_gather(basis_out, 'fs', axis=0, tiled=True)  45.9 us
    all_gather x1, waiting for transfers between devices, body(): whole_step = lax.all_gather(stepping, 'fs', axis=0, tiled=True)  41.8 us
    psum x1, blocking collectives, body(): total = lax.psum(jnp.sum(lowrank * lowrank), ('fs', 'tp'))  40 us
    all_gather x1, waiting for transfers between devices, body(): lax.all_gather(basis_in, 'fs', axis=0, tiled=True)  38.1 us
    unnamed x12, local copies, waits for them, and re-layouts  11.5 us
  transfers between devices with their start and end apart: 6, of which 6 were waited for; matrix products, arithmetic and copies ran while one was open for 5% of the time, Pallas kernels for 0%

commit v1 on v0

--- a/solution.py
+++ b/solution.py
@@ -52,7 +52,12 @@
     moments = 0.8 * jnp.concatenate([moment_in, moment_out], axis=1) + 0.2 * grads
     seconds = 0.9 * jnp.concatenate([second_in, second_out], axis=1) + 0.1 * grads * grads
     stepping = moments / (jnp.sqrt(seconds) + 1e-08)
-    whole_step = lax.all_gather(stepping, "fs", axis=0, tiled=True)
+    ring = [stepping]
+    for hop in range(15):
+        ring.append(lax.ppermute(ring[-1], "fs", [(dev, (dev + 1) % 16) for dev in range(16)]))
+    whole_step = jnp.roll(
+        jnp.concatenate(ring[::-1], axis=0), (lax.axis_index("fs") + 1) * ring[0].shape[0], axis=0
+    )
     update_in = jnp.dot(
         basis_in.astype(jnp.float32), whole_step[:, :units], precision=lax.Precision.HIGHEST
     )

time: 378 us -> 470 us (1.24)
  waiting for transfers between devices: 284 us -> 351 us
  local copies, waits for them, and re-layouts: 13.1 us -> 39.2 us
    ppermute x0 -> x15, waiting for transfers between devices: none -> 109 us  [body(): lax.ppermute(ring[-1], 'fs', [(dev, (dev + 1) % 16) for dev in range(16)])]
    all_gather x1 -> x0, waiting for transfers between devices: 41.8 us -> none  [body(): whole_step = lax.all_gather(stepping, 'fs', axis=0, tiled=True)]
    unnamed x12 -> x99, local copies, waits for them, and re-layouts: 11.5 us -> 37.5 us
  transfers between devices with their start and end apart: 6 -> 20, of which waited for: 6 -> 20; matrix products, arithmetic and copies ran while one was open for 5% -> 4% of each run, Pallas kernels for 0% -> 0%
where the time goes in v1:
time: 470 us; the launch traced here: 469 us
  waiting for transfers between devices  351 us (75%)
  blocking collectives  40 us (9%)
  local copies, waits for them, and re-layouts  39.2 us (8%)
  matrix products  16.5 us (4%)
  between operations  14.9 us (3%)
  other arithmetic  7.34 us (2%)
    ppermute x15, waiting for transfers between devices, body(): lax.ppermute(ring[-1], 'fs', [(dev, (dev + 1) % 16) for dev in range(16)])  109 us
    reduce_scatter x1, waiting for transfers between devices, body(): lax.psum_scatter(jnp.concatenate([term_in, term_out], axis=1), 'fs', scat...  62 us
    all_gather x1, waiting for transfers between devices, body(): lax.all_gather(weight_in_new.astype(jnp.bfloat16), 'fs', axis=0, tiled=True)  47.8 us
    all_gather x1, waiting for transfers between devices, body(): lax.all_gather(weight_out_new.astype(jnp.bfloat16), 'fs', axis=1, tiled=T...  46.4 us
    all_gather x1, waiting for transfers between devices, body(): lax.all_gather(basis_out, 'fs', axis=0, tiled=True)  45.9 us
    psum x1, blocking collectives, body(): total = lax.psum(jnp.sum(lowrank * lowrank), ('fs', 'tp'))  40 us
    all_gather x1, waiting for transfers between devices, body(): lax.all_gather(basis_in, 'fs', axis=0, tiled=True)  38.1 us
    unnamed x99, local copies, waits for them, and re-layouts  37.5 us
  transfers between devices with their start and end apart: 20, of which 20 were waited for; matrix products, arithmetic and copies ran while one was open for 4% of the time, Pallas kernels for 0%

profile of v1, /device:TPU:0, one launch (start us, length us, event | category | flops | bytes accessed | tf_op | source)
XLA Modules:
  0.0 469.2 jit_solution(163097248993950104)
XLA Ops:
  9.4 45.9 %all-gather.7.cloned.1.call-done = bf16[3072,384]{1,0:T(8,128)(2,1)} async-done(((bf16[192,384]{1,0:T(8,128)(2,1)}), bf16[3072,384]{1,0:T(8,128)(2,1)}) %all-gather.7.cloned.1.call-update) | async-done | bytes 2359312 | tf_op jit(solution)/shard_map/all_gather | solution.py:32
  55.3 5.2 %fusion.6 = f32[384,768]{1,0:T(8,128)} fusion(bf16[512,768]{1,0:T(8,128)(2,1)} %param.16, bf16[512,3072]{1,0:T(8,128)(2,1)S(1)} %copy-done, bf16[3072,384]{1,0:T(8,128)(2,1)} %all-gather.7.cloned.1.call-done), kind=kOutput, calls=%fused_computation.12 | convolution fusion | flops 1510146048 | bytes 7471104 | tf_op jit(solution)/shard_map/dot_general | solution.py:43
  60.5 38.1 %all-gather.5.cloned.1.call-done = bf16[3072,384]{1,0:T(8,128)(2,1)} async-done(((bf16[192,384]{1,0:T(8,128)(2,1)}), bf16[3072,384]{1,0:T(8,128)(2,1)}) %all-gather.5.cloned.1.call-update) | async-done | bytes 2359312 | tf_op jit(solution)/shard_map/all_gather | solution.py:31
  98.7 6.5 %fusion.5 = f32[384,768]{1,0:T(8,128)} fusion(bf16[512,3072]{1,0:T(8,128)(2,1)} %param.14, bf16[3072,384]{1,0:T(8,128)(2,1)} %all-gather.5.cloned.1.call-done, bf16[512,768]{1,0:T(8,128)(2,1)} %param.17, bf16[512,768]{1,0:T(8,128)(2,1)} %param.18, f32[768]{0:T(1024)S(1)} %broadcast_subtract_fusion), kind=kOutput, calls=%fused_computation.11 | convolution fusion | flops 1514078208 | bytes 8260608 | tf_op jit(solution)/shard_map/dot_general | solution.py:42
  108.6 62.0 %reduce-scatter.2.cloned.1.call-done = f32[24,1536]{1,0:T(8,128)} async-done(((f32[384,1536]{1,0:T(8,128)}), f32[24,1536]{1,0:T(8,128)}) %reduce-scatter.2.cloned.1.call-update) | async-done | bytes 147472 | tf_op jit(solution)/shard_map/reduce_scatter | solution.py:46
  172.1 40.0 %psum.7 = f32[]{:T(128)} all-reduce(f32[]{:T(128)} %multiply_reduce_fusion), channel_id=1, replica_groups=mesh['fs'=16,'tp'=2] {'fs','tp'}, use_global_device_ids=true, to_apply=%region_2.0 | all-reduce | flops 1 | bytes 8 | tf_op jit(solution)/shard_map/psum | solution.py:49
  214.6 7.3 %collective-permute-done = f32[24,1536]{1,0:T(8,128)S(1)} collective-permute-done((f32[24,1536]{1,0:T(8,128)S(1)}, f32[24,1536]{1,0:T(8,128)S(1)}, u32[]{:S(2)}, u32[]{:S(2)}) %collective-permute-start) | collective-permute-done | bytes 147488 | tf_op jit(solution)/shard_map/ppermute | solution.py:57
  222.6 7.3 %collective-permute-done.1 = f32[24,1536]{1,0:T(8,128)S(1)} collective-permute-done((f32[24,1536]{1,0:T(8,128)S(1)}, f32[24,1536]{1,0:T(8,128)S(1)}, u32[]{:S(2)}, u32[]{:S(2)}) %collective-permute-start.1) | collective-permute-done | bytes 147488 | tf_op jit(solution)/shard_map/ppermute | solution.py:57
  230.5 7.3 %collective-permute-done.2 = f32[24,1536]{1,0:T(8,128)S(1)} collective-permute-done((f32[24,1536]{1,0:T(8,128)S(1)}, f32[24,1536]{1,0:T(8,128)S(1)}, u32[]{:S(2)}, u32[]{:S(2)}) %collective-permute-start.2) | collective-permute-done | bytes 147488 | tf_op jit(solution)/shard_map/ppermute | solution.py:57
  238.4 7.3 %collective-permute-done.3 = f32[24,1536]{1,0:T(8,128)S(1)} collective-permute-done((f32[24,1536]{1,0:T(8,128)S(1)}, f32[24,1536]{1,0:T(8,128)S(1)}, u32[]{:S(2)}, u32[]{:S(2)}) %collective-permute-start.3) | collective-permute-done | bytes 147488 | tf_op jit(solution)/shard_map/ppermute | solution.py:57
  246.3 7.3 %collective-permute-done.4 = f32[24,1536]{1,0:T(8,128)S(1)} collective-permute-done((f32[24,1536]{1,0:T(8,128)S(1)}, f32[24,1536]{1,0:T(8,128)S(1)}, u32[]{:S(2)}, u32[]{:S(2)}) %collective-permute-start.4) | collective-permute-done | bytes 147488 | tf_op jit(solution)/shard_map/ppermute | solution.py:57
  253.6 7.3 %collective-permute-done.5 = f32[24,1536]{1,0:T(8,128)S(1)} collective-permute-done((f32[24,1536]{1,0:T(8,128)S(1)}, f32[24,1536]{1,0:T(8,128)S(1)}, u32[]{:S(2)}, u32[]{:S(2)}) %collective-permute-start.5) | collective-permute-done | bytes 147488 | tf_op jit(solution)/shard_map/ppermute | solution.py:57
  261.5 7.3 %collective-permute-done.6 = f32[24,1536]{1,0:T(8,128)S(1)} collective-permute-done((f32[24,1536]{1,0:T(8,128)S(1)}, f32[24,1536]{1,0:T(8,128)S(1)}, u32[]{:S(2)}, u32[]{:S(2)}) %collective-permute-start.6) | collective-permute-done | bytes 147488 | tf_op jit(solution)/shard_map/ppermute | solution.py:57
  269.4 7.3 %collective-permute-done.7 = f32[24,1536]{1,0:T(8,128)S(1)} collective-permute-done((f32[24,1536]{1,0:T(8,128)S(1)}, f32[24,1536]{1,0:T(8,128)S(1)}, u32[]{:S(2)}, u32[]{:S(2)}) %collective-permute-start.7) | collective-permute-done | bytes 147488 | tf_op jit(solution)/shard_map/ppermute | solution.py:57
  277.4 7.3 %collective-permute-done.8 = f32[24,1536]{1,0:T(8,128)S(1)} collective-permute-done((f32[24,1536]{1,0:T(8,128)S(1)}, f32[24,1536]{1,0:T(8,128)S(1)}, u32[]{:S(2)}, u32[]{:S(2)}) %collective-permute-start.8) | collective-permute-done | bytes 147488 | tf_op jit(solution)/shard_map/ppermute | solution.py:57
  285.3 7.3 %collective-permute-done.9 = f32[24,1536]{1,0:T(8,128)S(1)} collective-permute-done((f32[24,1536]{1,0:T(8,128)S(1)}, f32[24,1536]{1,0:T(8,128)S(1)}, u32[]{:S(2)}, u32[]{:S(2)}) %collective-permute-start.9) | collective-permute-done | bytes 147488 | tf_op jit(solution)/shard_map/ppermute | solution.py:57
  293.2 7.3 %collective-permute-done.10 = f32[24,1536]{1,0:T(8,128)S(1)} collective-permute-done((f32[24,1536]{1,0:T(8,128)S(1)}, f32[24,1536]{1,0:T(8,128)S(1)}, u32[]{:S(2)}, u32[]{:S(2)}) %collective-permute-start.10) | collective-permute-done | bytes 147488 | tf_op jit(solution)/shard_map/ppermute | solution.py:57
  301.2 7.3 %collective-permute-done.11 = f32[24,1536]{1,0:T(8,128)S(1)} collective-permute-done((f32[24,1536]{1,0:T(8,128)S(1)}, f32[24,1536]{1,0:T(8,128)S(1)}, u32[]{:S(2)}, u32[]{:S(2)}) %collective-permute-start.11) | collective-permute-done | bytes 147488 | tf_op jit(solution)/shard_map/ppermute | solution.py:57
  309.1 7.3 %collective-permute-done.12 = f32[24,1536]{1,0:T(8,128)S(1)} collective-permute-done((f32[24,1536]{1,0:T(8,128)S(1)}, f32[24,1536]{1,0:T(8,128)S(1)}, u32[]{:S(2)}, u32[]{:S(2)}) %collective-permute-start.12) | collective-permute-done | bytes 147488 | tf_op jit(solution)/shard_map/ppermute | solution.py:57
  317.0 7.4 %collective-permute-done.13 = f32[24,1536]{1,0:T(8,128)} collective-permute-done((f32[24,1536]{1,0:T(8,128)S(1)}, f32[24,1536]{1,0:T(8,128)}, u32[]{:S(2)}, u32[]{:S(2)}) %collective-permute-start.13) | collective-permute-done | bytes 147488 | tf_op jit(solution)/shard_map/ppermute | solution.py:57
  324.5 7.5 %collective-permute-done.14 = f32[24,1536]{1,0:T(8,128)} collective-permute-done((f32[24,1536]{1,0:T(8,128)}, f32[24,1536]{1,0:T(8,128)}, u32[]{:S(2)}, u32[]{:S(2)}) %collective-permute-start.14) | collective-permute-done | bytes 147488 | tf_op jit(solution)/shard_map/ppermute | solution.py:57
  357.0 46.4 %all-gather.11.cloned.1.call-done = bf16[768,3072]{0,1:T(8,128)(2,1)} async-done(((bf16[768,192]{0,1:T(8,128)(2,1)}), bf16[768,3072]{0,1:T(8,128)(2,1)}) %all-gather.11.cloned.1.call-update) | async-done | bytes 4718608 | tf_op jit(solution)/shard_map/all_gather | solution.py:71
  403.5 6.6 %copy.22 = bf16[768,3072]{1,0:T(8,128)(2,1)} copy(bf16[768,3072]{0,1:T(8,128)(2,1)} %all-gather.11.cloned.1.call-done) | data formatting | bytes 9437184
  410.1 47.8 %all-gather.9.cloned.1.call-done = bf16[3072,768]{1,0:T(8,128)(2,1)} async-done(((bf16[192,768]{1,0:T(8,128)(2,1)}), bf16[3072,768]{1,0:T(8,128)(2,1)}) %all-gather.9.cloned.1.call-update) | async-done | bytes 4718608 | tf_op jit(solution)/shard_map/all_gather | solution.py:70
  (131 shorter events, 46.5 us)
Async XLA Ops:
  7.2 48.2 %all-gather.7.cloned.1.call-start = ((), (), s32[]{:S(2)}) async-start(), calls=%async_computation.2 | async-start | bytes 2506752 | tf_op jit(solution)/shard_map/all_gather | solution.py:32
  7.9 90.8 %all-gather.5.cloned.1.call-start = ((), (), s32[]{:S(2)}) async-start(), calls=%async_computation.1 | async-start | bytes 2506752 | tf_op jit(solution)/shard_map/all_gather | solution.py:31
  8.7 161.9 %reduce-scatter.2.cloned.1.call-start = ((), (), s32[]{:S(2)}) async-start(), calls=%async_computation.3 | async-start | bytes 2506752 | tf_op jit(solution)/shard_map/reduce_scatter | solution.py:46
  105.2 107.7 %copy-start.30 = (f32[24,768]{1,0:T(8,128)S(1)}, f32[24,768]{1,0:T(8,128)}, u32[]{:S(2)}) copy-start(f32[24,768]{1,0:T(8,128)} %param.25) | copy-start | bytes 221188
  105.2 107.7 %copy-start.31 = (f32[24,768]{1,0:T(8,128)S(1)}, f32[24,768]{1,0:T(8,128)}, u32[]{:S(2)}) copy-start(f32[24,768]{1,0:T(8,128)} %param.23) | copy-start | bytes 221188
  105.2 107.7 %copy-start.32 = (f32[24,768]{1,0:T(8,128)S(1)}, f32[24,768]{1,0:T(8,128)}, u32[]{:S(2)}) copy-start(f32[24,768]{1,0:T(8,128)} %param.24) | copy-start | bytes 221188
  108.5 295.0 %all-gather.11.cloned.1.call-start = ((), (), s32[]{:S(2)}) async-start(), calls=%async_computation.5 | async-start | bytes 5013504 | tf_op jit(solution)/shard_map/all_gather | solution.py:71
  214.6 7.3 %collective-permute-start = (f32[24,1536]{1,0:T(8,128)S(1)}, f32[24,1536]{1,0:T(8,128)S(1)}, u32[]{:S(2)}, u32[]{:S(2)}) collective-permute-start(f32[24,1536]{1,0:T(8,128)S(1)} %get-tuple-element.16), channel_id=1, source_target_pairs={{0,2},{2,4},{4,6},{6,8},{8,10},{10,12},{12,14},{14,16},{16,18},{18... | collective-permute-start | bytes 442376 | tf_op jit(solution)/shard_map/ppermute | solution.py:57
  222.6 7.3 %collective-permute-start.1 = (f32[24,1536]{1,0:T(8,128)S(1)}, f32[24,1536]{1,0:T(8,128)S(1)}, u32[]{:S(2)}, u32[]{:S(2)}) collective-permute-start(f32[24,1536]{1,0:T(8,128)S(1)} %collective-permute-done), channel_id=1, source_target_pairs={{0,2},{2,4},{4,6},{6,8},{8,10},{10,12},{12,14},{14,16},{16,18},{18... | collective-permute-start | bytes 442376 | tf_op jit(solution)/shard_map/ppermute | solution.py:57
  230.5 7.3 %collective-permute-start.2 = (f32[24,1536]{1,0:T(8,128)S(1)}, f32[24,1536]{1,0:T(8,128)S(1)}, u32[]{:S(2)}, u32[]{:S(2)}) collective-permute-start(f32[24,1536]{1,0:T(8,128)S(1)} %collective-permute-done.1), channel_id=1, source_target_pairs={{0,2},{2,4},{4,6},{6,8},{8,10},{10,12},{12,14},{14,16},{16,18},{18... | collective-permute-start | bytes 442376 | tf_op jit(solution)/shard_map/ppermute | solution.py:57
  238.4 7.3 %collective-permute-start.3 = (f32[24,1536]{1,0:T(8,128)S(1)}, f32[24,1536]{1,0:T(8,128)S(1)}, u32[]{:S(2)}, u32[]{:S(2)}) collective-permute-start(f32[24,1536]{1,0:T(8,128)S(1)} %collective-permute-done.2), channel_id=1, source_target_pairs={{0,2},{2,4},{4,6},{6,8},{8,10},{10,12},{12,14},{14,16},{16,18},{18... | collective-permute-start | bytes 442376 | tf_op jit(solution)/shard_map/ppermute | solution.py:57
  246.3 7.3 %collective-permute-start.4 = (f32[24,1536]{1,0:T(8,128)S(1)}, f32[24,1536]{1,0:T(8,128)S(1)}, u32[]{:S(2)}, u32[]{:S(2)}) collective-permute-start(f32[24,1536]{1,0:T(8,128)S(1)} %collective-permute-done.3), channel_id=1, source_target_pairs={{0,2},{2,4},{4,6},{6,8},{8,10},{10,12},{12,14},{14,16},{16,18},{18... | collective-permute-start | bytes 442376 | tf_op jit(solution)/shard_map/ppermute | solution.py:57
  253.6 87.6 %copy-start.13 = (f32[24,1536]{1,0:T(8,128)}, f32[24,1536]{1,0:T(8,128)S(1)}, u32[]{:S(2)}) copy-start(f32[24,1536]{1,0:T(8,128)S(1)} %collective-permute-done.4) | copy-start | bytes 442372
  253.6 7.3 %collective-permute-start.5 = (f32[24,1536]{1,0:T(8,128)S(1)}, f32[24,1536]{1,0:T(8,128)S(1)}, u32[]{:S(2)}, u32[]{:S(2)}) collective-permute-start(f32[24,1536]{1,0:T(8,128)S(1)} %collective-permute-done.4), channel_id=1, source_target_pairs={{0,2},{2,4},{4,6},{6,8},{8,10},{10,12},{12,14},{14,16},{16,18},{18... | collective-permute-start | bytes 442376 | tf_op jit(solution)/shard_map/ppermute | solution.py:57
  261.5 7.3 %collective-permute-start.6 = (f32[24,1536]{1,0:T(8,128)S(1)}, f32[24,1536]{1,0:T(8,128)S(1)}, u32[]{:S(2)}, u32[]{:S(2)}) collective-permute-start(f32[24,1536]{1,0:T(8,128)S(1)} %collective-permute-done.5), channel_id=1, source_target_pairs={{0,2},{2,4},{4,6},{6,8},{8,10},{10,12},{12,14},{14,16},{16,18},{18... | collective-permute-start | bytes 442376 | tf_op jit(solution)/shard_map/ppermute | solution.py:57
  269.4 7.3 %collective-permute-start.7 = (f32[24,1536]{1,0:T(8,128)S(1)}, f32[24,1536]{1,0:T(8,128)S(1)}, u32[]{:S(2)}, u32[]{:S(2)}) collective-permute-start(f32[24,1536]{1,0:T(8,128)S(1)} %collective-permute-done.6), channel_id=1, source_target_pairs={{0,2},{2,4},{4,6},{6,8},{8,10},{10,12},{12,14},{14,16},{16,18},{18... | collective-permute-start | bytes 442376 | tf_op jit(solution)/shard_map/ppermute | solution.py:57
  277.4 7.3 %collective-permute-start.8 = (f32[24,1536]{1,0:T(8,128)S(1)}, f32[24,1536]{1,0:T(8,128)S(1)}, u32[]{:S(2)}, u32[]{:S(2)}) collective-permute-start(f32[24,1536]{1,0:T(8,128)S(1)} %collective-permute-done.7), channel_id=1, source_target_pairs={{0,2},{2,4},{4,6},{6,8},{8,10},{10,12},{12,14},{14,16},{16,18},{18... | collective-permute-start | bytes 442376 | tf_op jit(solution)/shard_map/ppermute | solution.py:57
  285.3 7.3 %collective-permute-start.9 = (f32[24,1536]{1,0:T(8,128)S(1)}, f32[24,1536]{1,0:T(8,128)S(1)}, u32[]{:S(2)}, u32[]{:S(2)}) collective-permute-start(f32[24,1536]{1,0:T(8,128)S(1)} %collective-permute-done.8), channel_id=1, source_target_pairs={{0,2},{2,4},{4,6},{6,8},{8,10},{10,12},{12,14},{14,16},{16,18},{18... | collective-permute-start | bytes 442376 | tf_op jit(solution)/shard_map/ppermute | solution.py:57
  293.2 7.3 %collective-permute-start.10 = (f32[24,1536]{1,0:T(8,128)S(1)}, f32[24,1536]{1,0:T(8,128)S(1)}, u32[]{:S(2)}, u32[]{:S(2)}) collective-permute-start(f32[24,1536]{1,0:T(8,128)S(1)} %collective-permute-done.9), channel_id=1, source_target_pairs={{0,2},{2,4},{4,6},{6,8},{8,10},{10,12},{12,14},{14,16},{16,18},{18... | collective-permute-start | bytes 442376 | tf_op jit(solution)/shard_map/ppermute | solution.py:57
  301.1 7.3 %collective-permute-start.11 = (f32[24,1536]{1,0:T(8,128)S(1)}, f32[24,1536]{1,0:T(8,128)S(1)}, u32[]{:S(2)}, u32[]{:S(2)}) collective-permute-start(f32[24,1536]{1,0:T(8,128)S(1)} %collective-permute-done.10), channel_id=1, source_target_pairs={{0,2},{2,4},{4,6},{6,8},{8,10},{10,12},{12,14},{14,16},{16,18},{18... | collective-permute-start | bytes 442376 | tf_op jit(solution)/shard_map/ppermute | solution.py:57
  309.1 7.3 %collective-permute-start.12 = (f32[24,1536]{1,0:T(8,128)S(1)}, f32[24,1536]{1,0:T(8,128)S(1)}, u32[]{:S(2)}, u32[]{:S(2)}) collective-permute-start(f32[24,1536]{1,0:T(8,128)S(1)} %collective-permute-done.11), channel_id=1, source_target_pairs={{0,2},{2,4},{4,6},{6,8},{8,10},{10,12},{12,14},{14,16},{16,18},{18... | collective-permute-start | bytes 442376 | tf_op jit(solution)/shard_map/ppermute | solution.py:57
  317.0 7.4 %collective-permute-start.13 = (f32[24,1536]{1,0:T(8,128)S(1)}, f32[24,1536]{1,0:T(8,128)}, u32[]{:S(2)}, u32[]{:S(2)}) collective-permute-start(f32[24,1536]{1,0:T(8,128)S(1)} %collective-permute-done.12), channel_id=1, source_target_pairs={{0,2},{2,4},{4,6},{6,8},{8,10},{10,12},{12,14},{14,16},{16,18},{18... | collective-permute-start | bytes 442376 | tf_op jit(solution)/shard_map/ppermute | solution.py:57
  324.4 7.6 %collective-permute-start.14 = (f32[24,1536]{1,0:T(8,128)}, f32[24,1536]{1,0:T(8,128)}, u32[]{:S(2)}, u32[]{:S(2)}) collective-permute-start(f32[24,1536]{1,0:T(8,128)} %collective-permute-done.13), channel_id=1, source_target_pairs={{0,2},{2,4},{4,6},{6,8},{8,10},{10,12},{12,14},{14,16},{16,18},{18... | collective-permute-start | bytes 442376 | tf_op jit(solution)/shard_map/ppermute | solution.py:57
  352.2 105.7 %all-gather.9.cloned.1.call-start = ((), (), s32[]{:S(2)}) async-start(), calls=%async_computation.4 | async-start | bytes 5013504 | tf_op jit(solution)/shard_map/all_gather | solution.py:70
  (29 other events, 396.1 us)
Sparse Core Ops, SparseCore 0:
  10.3 45.0 all-gather.6
  57.6 41.0 all-gather.4
  108.6 61.9 reduce-scatter.1
  352.3 51.1 all-gather.10
  406.2 51.6 all-gather.8
